TPU v7x, 128 devices: a whole 4x4x4 slice. The times are simulated.
128 devices in a mesh: rep: 4 (over z), fs: 4 (over y), tp: 8 (over x, core).
Axes of the slice: x: 4, y: 4, z: 4, core: 2. Of those that a mesh axis runs over, the one named last changes fastest.
Arguments:
- tokens_in: bfloat16 [12288, 1024], P(('rep', 'fs', 'tp')), may hold values from -6 to 6
- out_grad: bfloat16 [12288, 1024], P(('rep', 'fs', 'tp')), may hold values from -24 to 24
- gate_weight: bfloat16 [1024, 2816], P('fs', 'tp'), may hold values from -0.1875 to 0.1875
- up_weight: bfloat16 [1024, 2816], P('fs', 'tp'), may hold values from -0.1875 to 0.1875
- down_weight: bfloat16 [2816, 1024], P('tp', 'fs'), may hold values from -0.109375 to 0.109375
Outputs:
- grad_in: bfloat16 [12288, 1024], P(('rep', 'fs', 'tp'))
- grad_gate_w: float32 [1024, 2816], P('fs', 'tp')
- grad_up_w: float32 [1024, 2816], P('fs', 'tp')
- grad_down_w: float32 [2816, 1024], P('tp', 'fs')
All inputs are finite; a program needn't handle non-finite values.
Results may differ from a plain program's by a relative error of at most 0.02.
Values may be sent and summed in bfloat16 or wider, within the bound.
No kernel may reach another device: no remote copies, remote signals or barrier semaphores. Data moves between devices by JAX's collectives and lax.ppermute only.
A program may use at most 64 MiB of HBM per device.

v0:
```python
import jax
import jax.numpy as jnp
from jax import lax
from jax.experimental import pallas as pl
from jax.experimental.pallas import tpu as pltpu
from jax.sharding import Mesh, PartitionSpec as P


BF = jnp.bfloat16
F32 = jnp.float32

UP = [(2 * i + c, 2 * ((i + (1, 3)[c]) % 4) + c) for i in range(4) for c in range(2)]
DOWN = [(b, a) for a, b in UP]
PAIRS = [(2 * i + c, 2 * ((i ^ 1, 3 - i)[c]) + c) for i in range(4) for c in range(2)]
CROSS = [(2 * i + c, 2 * ((3 - i, i ^ 1)[c]) + c) for i in range(4) for c in range(2)]
SWAP = [(0, 1), (1, 0)]


def nt(a, b):
    return lax.dot_general(a, b, (((1,), (1,)), ((), ())), preferred_element_type=F32)


def nn(a, b):
    return lax.dot_general(a, b, (((1,), (0,)), ((), ())), preferred_element_type=F32)


def tn(a, b):
    return lax.dot_general(a, b, (((0,), (0,)), ((), ())), preferred_element_type=F32)


def columns_of(width):
    f = lax.axis_index("fs")
    step = 1 - 2 * lax.axis_index("tc")
    return [
        pl.ds(pl.multiple_of(((f + d) % 4) * width, width), width)
        for d in (0, 4 - step, 4 + step, 2)
    ]


def pack_kernel(x, g, wg, wu, wd, xg, w, sems):
    rows, hid = x.shape[0], wg.shape[0]
    places = (
        (wg, w.at[:hid]),
        (wu, w.at[hid : 2 * hid]),
        (wd, w.at[2 * hid :]),
        (x, xg.at[:rows]),
        (g, xg.at[rows:]),
    )
    copies = [pltpu.make_async_copy(a, b, sems.at[i]) for i, (a, b) in enumerate(places)]
    for copy in copies:
        copy.start()
    for copy in copies:
        copy.wait()


def forward_kernel(factor, *refs):
    blocks, weights = refs[:8], refs[8:12]
    xs, gs, gate_t, up_t, wg, wu, wd, own, behind, ahead, far = refs[12:]
    rows = blocks[0].shape[0] // 2
    hid, width = own.shape
    places = columns_of(width)
    for i, b in enumerate(blocks):
        xs[i * rows : (i + 1) * rows] = b[:rows]
        gs[i * rows : (i + 1) * rows] = b[rows:]
    for ref, cols in zip(weights, places):
        wg[:, cols] = ref[:hid]
        wu[:, cols] = ref[hid : 2 * hid]
        wd[:, cols] = ref[2 * hid :]
    gate = nt(wg[...], xs[...]).astype(BF)
    up = nt(wu[...], xs[...]).astype(BF)
    gate_t[...] = gate
    up_t[...] = up
    wide = gate.astype(F32)
    hidden = (wide * jax.nn.sigmoid(wide) * up.astype(F32)).astype(BF)
    for out, cols in zip((own, behind, ahead, far), places):
        out[...] = (factor * nn(hidden, gs[:, cols])).astype(BF)


def backward_kernel(factor, xs, gs, gate_t, up_t, wd, gg_t, gu_t, *outs):
    hid = wd.shape[0]
    grad = nt(wd[...], gs[...]).astype(BF).astype(F32)
    gate = gate_t[...].astype(F32)
    up = up_t[...].astype(F32)
    sig = jax.nn.sigmoid(gate)
    grad_gate = (grad * up * sig * (1.0 + gate * (1.0 - sig))).astype(BF)
    grad_up = (grad * (gate * sig)).astype(BF)
    gg_t[...] = grad_gate
    gu_t[...] = grad_up
    for out, cols in zip(outs, columns_of(outs[0].shape[1])):
        x = xs[:, cols]
        out[:hid] = (factor * nn(grad_gate, x)).astype(BF)
        out[hid:] = (factor * nn(grad_up, x)).astype(BF)


def input_kernel(gg_t, gu_t, wg, wu, mine, other):
    half = mine.shape[0]
    mine[...] = tn(gg_t[:, :half], wg[...]) + tn(gu_t[:, :half], wu[...])
    other[...] = (tn(gg_t[:, half:], wg[...]) + tn(gu_t[:, half:], wu[...])).astype(BF)


def pair_kernel(mine, other, own, behind, far, ahead):
    rows = own.shape[0]
    for i, out in enumerate((own, behind, far, ahead)):
        part = slice(i * rows, (i + 1) * rows)
        out[...] = (mine[part] + other[part].astype(F32)).astype(out.dtype)


def outputs_kernel(own, behind, ahead, down_a, down_b, grad_in, down):
    grad_in[...] = (own[...] + behind[...].astype(F32) + ahead[...].astype(F32)).astype(BF)
    down[...] = down_a[...].astype(F32) + down_b[...].astype(F32)


def weights_kernel(a, b, gate, up):
    hid = gate.shape[0]
    gate[...] = a[:hid].astype(F32) + b[:hid].astype(F32)
    up[...] = a[hid:].astype(F32) + b[hid:].astype(F32)


def call(kernel, outs, *args, inputs=pltpu.VMEM, outputs=pltpu.VMEM, scratch=()):
    inside = pl.BlockSpec(memory_space=pltpu.VMEM)
    given = pl.BlockSpec(memory_space=inputs)
    args = [pltpu.with_memory_space_constraint(a, inputs) for a in args]
    return pl.pallas_call(
        kernel,
        out_shape=[outputs(*o) if outputs else jax.ShapeDtypeStruct(*o) for o in outs],
        in_specs=[given] * len(args),
        out_specs=[inside] * len(outs),
        scratch_shapes=list(scratch),
        compiler_params=pltpu.CompilerParams(vmem_limit_bytes=16 * 2**20),
    )(*args)


def swap(value):
    return lax.ppermute(value, "tc", SWAP)


def plus(a, b):
    return (a.astype(F32) + b.astype(F32)).astype(BF)


def body(tokens_in, out_grad, gate_weight, up_weight, down_weight):
    rows, model = tokens_in.shape
    width, hid = gate_weight.shape
    toks = 8 * rows
    factor = (toks * 16) ** (-0.5)
    x_axis, y_axis, z_axis = ("tx", "tc"), ("fs", "tc"), ("rep", "tc")
    xg, w = call(
        pack_kernel,
        [((2 * rows, model), BF), ((3 * hid, width), BF)],
        tokens_in,
        out_grad,
        gate_weight.T,
        up_weight.T,
        down_weight,
        inputs=pltpu.HBM,
        scratch=[pltpu.SemaphoreType.DMA((5,))],
    )
    w_behind = lax.ppermute(w, y_axis, UP)
    x_behind = lax.ppermute(xg, x_axis, UP)
    w_other, x_other = swap(w), swap(xg)
    w_second = lax.ppermute(w_other, y_axis, UP)
    x_second = lax.ppermute(x_other, x_axis, UP)
    w_far = lax.ppermute(w_behind, y_axis, UP)
    x_far = lax.ppermute(x_behind, x_axis, UP)
    w_ahead = swap(w_second)
    blocks = [xg, x_behind, x_far, swap(x_second), x_other, swap(x_behind), swap(x_far), x_second]
    big = ((toks, model), BF)
    hidden_shape = ((hid, toks), BF)
    weight = ((hid, model), BF)
    xs, gs, gate_t, up_t, wg, wu, wd, *downs = call(
        lambda *r: forward_kernel(factor, *r),
        [big, big, hidden_shape, hidden_shape, weight, weight, weight] + [((hid, width), BF)] * 4,
        *blocks,
        w,
        w_behind,
        w_ahead,
        w_far,
    )

    def scattered(axes, own, behind, ahead, far):
        relayed = lax.ppermute(far, axes, UP)
        back = lax.ppermute(behind, axes, DOWN)
        front = lax.ppermute(plus(ahead, relayed), axes, UP)
        return own, back, front

    def reduced(own, back, front):
        part = (own.astype(F32) + back.astype(F32) + front.astype(F32)).astype(BF)
        pair = plus(part, lax.ppermute(part, z_axis, PAIRS))
        return pair, lax.ppermute(pair, z_axis, CROSS)

    down = reduced(*scattered(y_axis, *downs))
    gg_t, gu_t, *parts = call(
        lambda *r: backward_kernel(factor, *r),
        [hidden_shape, hidden_shape] + [((2 * hid, width), BF)] * 4,
        xs,
        gs,
        gate_t,
        up_t,
        wd,
    )
    both = reduced(*scattered(y_axis, *parts))
    half = ((toks // 2, model),)
    kept, given = call(input_kernel, [half + (F32,), half + (BF,)], gg_t, gu_t, wg, wu)
    piece = (rows, model)
    own, behind, far, ahead = call(
        pair_kernel, [(piece, F32)] + [(piece, BF)] * 3, kept, swap(given)
    )
    grad_parts = scattered(x_axis, own, behind, ahead, far)
    grad_in, grad_down = call(
        outputs_kernel, [(piece, BF), ((hid, width), F32)], *grad_parts, *down, outputs=None
    )
    grad_gate, grad_up = call(weights_kernel, [((hid, width), F32)] * 2, *both, outputs=None)
    return (grad_in, grad_gate.T, grad_up.T, grad_down)


def solution(mesh):
    split = Mesh(mesh.devices.reshape(4, 4, 4, 2), ("rep", "fs", "tx", "tc"))
    tokens = P(("rep", "fs", "tx", "tc"), None)
    columns = P("fs", ("tx", "tc"))
    lines = P(("tx", "tc"), "fs")
    return jax.shard_map(
        body,
        mesh=split,
        in_specs=(tokens, tokens, columns, columns, lines),
        out_specs=(tokens, columns, columns, lines),
        check_vma=False,
    )
```

profile of v0, /device:TPU:0, one launch (start us, length us, event | category | flops | bytes accessed | tf_op | source)
XLA Modules:
  0.0 76.6 jit_solution(407371575610926669)
XLA Ops:
  0.6 1.3 %shard_map.84 = (bf16[192,1024]{1,0:T(8,128)(2,1)S(1)}, bf16[1056,256]{1,0:T(8,128)(2,1)S(1)}) custom-call(bf16[96,1024]{1,0:T(8,128)(2,1)} %x.1, bf16[96,1024]{1,0:T(8,128)(2,1)} %g.1, bf16[352,256]{1,0:T(8,128)(2,1)} %bitcast.4, bf16[352,256]{1,0:T(8,128)(2,1)} %bitcast.5, bf16[352,256]{1,0:T(8,128)(2,1)} %wd.1), custom_call_target="tpu_custom_call" | custom-call | tf_op jit(solution)/shard_map/pallas_call | solution.py:123
  1.9 0.1 collective-permute-start.8
  2.0 0.5 collective-permute-start.2
  2.5 1.6 %collective-permute-start = (bf16[192,1024]{1,0:T(8,128)(2,1)S(1)}, bf16[192,1024]{1,0:T(8,128)(2,1)S(1)}, u32[]{:S(2)}, u32[]{:S(2)}) collective-permute-start(bf16[192,1024]{1,0:T(8,128)(2,1)S(1)} %get-tuple-element.33.r_0_), channel_id=1, source_target_pairs={{0,2},{1,7},{2,4},{3,1},{4,6},{5,3},{6,0},{7,5},{8,10},{9,15},{10,... | collective-permute-start | bytes 1179656 | tf_op jit(solution)/shard_map/ppermute | solution.py:159
  4.1 1.6 %collective-permute-start.7 = (bf16[1056,256]{1,0:T(8,128)(2,1)S(1)}, bf16[1056,256]{1,0:T(8,128)(2,1)S(1)}, u32[]{:S(2)}, u32[]{:S(2)}) collective-permute-start(bf16[1056,256]{1,0:T(8,128)(2,1)S(1)} %get-tuple-element.34.r_8_), channel_id=1, source_target_pairs={{0,8},{1,25},{8,16},{9,1},{16,24},{17,9},{24,0},{25,17},{2,10},{3,... | collective-permute-start | bytes 1622024 | tf_op jit(solution)/shard_map/ppermute | solution.py:158
  5.7 0.0 collective-permute-done.8
  5.7 1.6 %collective-permute-start.9 = (bf16[1056,256]{1,0:T(8,128)(2,1)S(1)}, bf16[1056,256]{1,0:T(8,128)(2,1)S(1)}, u32[]{:S(2)}, u32[]{:S(2)}) collective-permute-start(bf16[1056,256]{1,0:T(8,128)(2,1)S(1)} %collective-permute-done.8), channel_id=1, source_target_pairs={{0,8},{1,25},{8,16},{9,1},{16,24},{17,9},{24,0},{25,17},{2,10},{3,... | collective-permute-start | bytes 1622024 | tf_op jit(solution)/shard_map/ppermute | solution.py:161
  7.3 1.5 %collective-permute-start.3 = (bf16[192,1024]{1,0:T(8,128)(2,1)S(1)}, bf16[192,1024]{1,0:T(8,128)(2,1)S(1)}, u32[]{:S(2)}, u32[]{:S(2)}) collective-permute-start(bf16[192,1024]{1,0:T(8,128)(2,1)S(1)} %collective-permute-done.2.r_4_), channel_id=1, source_target_pairs={{0,2},{1,7},{2,4},{3,1},{4,6},{5,3},{6,0},{7,5},{8,10},{9,15},{10,... | collective-permute-start | bytes 1179656 | tf_op jit(solution)/shard_map/ppermute | solution.py:162
  8.8 2.7 %collective-permute-done.r_1_ = bf16[192,1024]{1,0:T(8,128)(2,1)S(1)} collective-permute-done((bf16[192,1024]{1,0:T(8,128)(2,1)S(1)}, bf16[192,1024]{1,0:T(8,128)(2,1)S(1)}, u32[]{:S(2)}, u32[]{:S(2)}) %collective-permute-start) | collective-permute-done | bytes 393248 | tf_op jit(solution)/shard_map/ppermute | solution.py:159
  11.5 0.4 collective-permute-start.1
  11.9 2.8 %collective-permute-done.7.r_9_ = bf16[1056,256]{1,0:T(8,128)(2,1)S(1)} collective-permute-done((bf16[1056,256]{1,0:T(8,128)(2,1)S(1)}, bf16[1056,256]{1,0:T(8,128)(2,1)S(1)}, u32[]{:S(2)}, u32[]{:S(2)}) %collective-permute-start.7) | collective-permute-done | bytes 540704 | tf_op jit(solution)/shard_map/ppermute | solution.py:158
  14.7 0.4 collective-permute-start.11
  15.1 5.4 %collective-permute-done.9 = bf16[1056,256]{1,0:T(8,128)(2,1)S(1)} collective-permute-done((bf16[1056,256]{1,0:T(8,128)(2,1)S(1)}, bf16[1056,256]{1,0:T(8,128)(2,1)S(1)}, u32[]{:S(2)}, u32[]{:S(2)}) %collective-permute-start.9) | collective-permute-done | bytes 540704 | tf_op jit(solution)/shard_map/ppermute | solution.py:161
  20.5 0.0 collective-permute-start.10
  20.5 0.5 collective-permute-start.5
  21.0 0.0 collective-permute-start.4
  21.0 0.5 collective-permute-start.6
  21.5 1.5 %collective-permute-done.5.r_5_ = bf16[192,1024]{1,0:T(8,128)(2,1)S(1)} collective-permute-done((bf16[192,1024]{1,0:T(8,128)(2,1)S(1)}, bf16[192,1024]{1,0:T(8,128)(2,1)S(1)}, u32[]{:S(2)}, u32[]{:S(2)}) %collective-permute-start.5) | collective-permute-done | bytes 393248 | tf_op jit(solution)/shard_map/ppermute | solution.py:134
  23.0 3.3 %collective-permute-done.11.r_11_ = bf16[1056,256]{1,0:T(8,128)(2,1)S(1)} collective-permute-done((bf16[1056,256]{1,0:T(8,128)(2,1)S(1)}, bf16[1056,256]{1,0:T(8,128)(2,1)S(1)}, u32[]{:S(2)}, u32[]{:S(2)}) %collective-permute-start.11) | collective-permute-done | bytes 540704 | tf_op jit(solution)/shard_map/ppermute | solution.py:163
  26.3 2.3 %shard_map.85 = (bf16[768,1024]{1,0:T(8,128)(2,1)S(1)}, bf16[768,1024]{1,0:T(8,128)(2,1)S(1)}, bf16[352,768]{1,0:T(8,128)(2,1)S(1)}, bf16[352,768]{1,0:T(8,128)(...) custom-call(bf16[192,1024]{1,0:T(8,128)(2,1)S(1)} %get-tuple-element, ...), custom_call_target="tpu_custom_call" | custom-call | tf_op jit(solution)/shard_map/pallas_call | solution.py:123
  28.6 2.4 %shard_map.86 = (bf16[352,768]{1,0:T(8,128)(2,1)S(1)}, bf16[352,768]{1,0:T(8,128)(2,1)S(1)}, bf16[704,256]{1,0:T(8,128)(2,1)S(1)}, bf16[704,256]{1,0:T(8,128)(2,...) custom-call(bf16[768,1024]{1,0:T(8,128)(2,1)S(1)} %get-tuple-element.35.r_0_, ...), custom_call_target="tpu_custom_call" | custom-call | tf_op jit(solution)/shard_map/pallas_call | solution.py:123
  31.0 0.4 collective-permute-start.22
  31.4 1.6 %collective-permute-start.17 = (bf16[352,256]{1,0:T(8,128)(2,1)S(1)}, bf16[352,256]{1,0:T(8,128)(2,1)S(1)}, u32[]{:S(2)}, u32[]{:S(2)}) collective-permute-start(bf16[352,256]{1,0:T(8,128)(2,1)S(1)} %get-tuple-element.53), channel_id=1, source_target_pairs={{0,8},{1,25},{8,16},{9,1},{16,24},{17,9},{24,0},{25,17},{2,10},{3,... | collective-permute-start | bytes 540680 | tf_op jit(solution)/shard_map/ppermute | solution.py:181
  33.0 1.7 %collective-permute-start.21 = (bf16[704,256]{1,0:T(8,128)(2,1)S(1)}, bf16[704,256]{1,0:T(8,128)(2,1)S(1)}, u32[]{:S(2)}, u32[]{:S(2)}) collective-permute-start(bf16[704,256]{1,0:T(8,128)(2,1)S(1)} %get-tuple-element.56), channel_id=1, source_target_pairs={{8,0},{25,1},{16,8},{1,9},{24,16},{9,17},{0,24},{17,25},{10,2},{27... | collective-permute-start | bytes 1081352 | tf_op jit(solution)/shard_map/ppermute | solution.py:182
  34.7 1.8 %shard_map.87 = (f32[384,1024]{1,0:T(8,128)S(1)}, bf16[384,1024]{1,0:T(8,128)(2,1)S(1)}) custom-call(bf16[352,768]{1,0:T(8,128)(2,1)S(1)} %get-tuple-element.40.gg_t, bf16[352,768]{1,0:T(8,128)(2,1)S(1)} %get-tuple-element.41.gu_t, bf16[352,1024]{1,0:T(8,128)(2,1)S(1)} %get-tuple-element.42.wg, bf16[352,1024]{1,0:T(8,128)(2,1)S(1)} %get-tuple-element.43.wu), custom_call_target="tpu_custom_call" | custom-call | tf_op jit(solution)/shard_map/pallas_call | solution.py:123
  36.5 0.6 collective-permute-start.12
  37.1 4.7 %collective-permute-done.22 = bf16[704,256]{1,0:T(8,128)(2,1)S(1)} collective-permute-done((bf16[704,256]{1,0:T(8,128)(2,1)S(1)}, bf16[704,256]{1,0:T(8,128)(2,1)S(1)}, u32[]{:S(2)}, u32[]{:S(2)}) %collective-permute-start.22) | collective-permute-done | bytes 360480 | tf_op jit(solution)/shard_map/ppermute | solution.py:181
  41.8 0.1 add_convert_fusion.2
  41.9 0.1 collective-permute-start.23
  42.0 3.2 %collective-permute-start.16 = (bf16[352,256]{1,0:T(8,128)(2,1)S(1)}, bf16[352,256]{1,0:T(8,128)(2,1)S(1)}, u32[]{:S(2)}, u32[]{:S(2)}) collective-permute-start(bf16[352,256]{1,0:T(8,128)(2,1)S(1)} %get-tuple-element.51), channel_id=1, source_target_pairs={{8,0},{25,1},{16,8},{1,9},{24,16},{9,17},{0,24},{17,25},{10,2},{27... | collective-permute-start | bytes 540680 | tf_op jit(solution)/shard_map/ppermute | solution.py:182
  45.2 0.3 collective-permute-done.17
  45.6 0.1 collective-permute-start.18
  45.7 6.9 %collective-permute-done.23 = bf16[704,256]{1,0:T(8,128)(2,1)S(1)} collective-permute-done((bf16[704,256]{1,0:T(8,128)(2,1)S(1)}, bf16[704,256]{1,0:T(8,128)(2,1)S(1)}, u32[]{:S(2)}, u32[]{:S(2)}) %collective-permute-start.23) | collective-permute-done | bytes 360480 | tf_op jit(solution)/shard_map/ppermute | solution.py:183
  52.5 0.1 add_convert_fusion.1
  52.7 2.2 %collective-permute-start.24 = (bf16[704,256]{1,0:T(8,128)(2,1)S(1)}, bf16[704,256]{1,0:T(8,128)(2,1)S(1)}, u32[]{:S(2)}, u32[]{:S(2)}) collective-permute-start(bf16[704,256]{1,0:T(8,128)(2,1)S(1)} %add_convert_fusion.1), channel_id=1, source_target_pairs={{0,32},{1,97},{32,0},{33,65},{64,96},{65,33},{96,64},{97,1},{2,34}... | collective-permute-start | bytes 1081352 | tf_op jit(solution)/shard_map/ppermute | solution.py:188
  54.8 0.1 shard_map.88
  55.0 1.0 %collective-permute-start.14 = (bf16[96,1024]{1,0:T(8,128)(2,1)S(1)}, bf16[96,1024]{1,0:T(8,128)(2,1)S(1)}, u32[]{:S(2)}, u32[]{:S(2)}) collective-permute-start(bf16[96,1024]{1,0:T(8,128)(2,1)S(1)} %get-tuple-element.49), channel_id=1, source_target_pairs={{0,2},{1,7},{2,4},{3,1},{4,6},{5,3},{6,0},{7,5},{8,10},{9,15},{10,... | collective-permute-start | bytes 589832 | tf_op jit(solution)/shard_map/ppermute | solution.py:181
  56.0 0.1 add_convert_fusion.5
  56.0 0.5 collective-permute-start.19
  56.5 2.0 %collective-permute-start.13 = (bf16[96,1024]{1,0:T(8,128)(2,1)S(1)}, bf16[96,1024]{1,0:T(8,128)(2,1)S(1)}, u32[]{:S(2)}, u32[]{:S(2)}) collective-permute-start(bf16[96,1024]{1,0:T(8,128)(2,1)S(1)} %get-tuple-element.47), channel_id=1, source_target_pairs={{2,0},{7,1},{4,2},{1,3},{6,4},{3,5},{0,6},{5,7},{10,8},{15,9},{12,... | collective-permute-start | bytes 589832 | tf_op jit(solution)/shard_map/ppermute | solution.py:182
  58.5 5.4 %collective-permute-done.14 = bf16[96,1024]{1,0:T(8,128)(2,1)S(1)} collective-permute-done((bf16[96,1024]{1,0:T(8,128)(2,1)S(1)}, bf16[96,1024]{1,0:T(8,128)(2,1)S(1)}, u32[]{:S(2)}, u32[]{:S(2)}) %collective-permute-start.14) | collective-permute-done | bytes 196640 | tf_op jit(solution)/shard_map/ppermute | solution.py:181
  64.0 0.1 collective-permute-start.15
  64.1 0.1 add_convert_fusion.a
  64.2 2.3 %collective-permute-start.25 = (bf16[704,256]{1,0:T(8,128)(2,1)S(1)}, bf16[704,256]{1,0:T(8,128)(2,1)S(1)}, u32[]{:S(2)}, u32[]{:S(2)}) collective-permute-start(bf16[704,256]{1,0:T(8,128)(2,1)S(1)} %add_convert_fusion.a), channel_id=1, source_target_pairs={{0,96},{1,33},{32,64},{33,1},{64,32},{65,97},{96,0},{97,65},{2,98}... | collective-permute-start | bytes 1081352 | tf_op jit(solution)/shard_map/ppermute | solution.py:189
  66.6 1.1 %collective-permute-start.20 = (bf16[352,256]{1,0:T(8,128)(2,1)S(1)}, bf16[352,256]{1,0:T(8,128)(2,1)S(1)}, u32[]{:S(2)}, u32[]{:S(2)}) collective-permute-start(bf16[352,256]{1,0:T(8,128)(2,1)S(1)} %add_convert_fusion.4.down_a), channel_id=1, source_target_pairs={{0,96},{1,33},{32,64},{33,1},{64,32},{65,97},{96,0},{97,65},{2,98}... | collective-permute-start | bytes 540680 | tf_op jit(solution)/shard_map/ppermute | solution.py:189
  67.6 7.2 %collective-permute-done.20.down_b = bf16[352,256]{1,0:T(8,128)(2,1)S(1)} collective-permute-done((bf16[352,256]{1,0:T(8,128)(2,1)S(1)}, bf16[352,256]{1,0:T(8,128)(2,1)S(1)}, u32[]{:S(2)}, u32[]{:S(2)}) %collective-permute-start.20) | collective-permute-done | bytes 180256 | tf_op jit(solution)/shard_map/ppermute | solution.py:189
  74.9 0.9 %shard_map.89 = (bf16[96,1024]{1,0:T(8,128)(2,1)}, f32[352,256]{1,0:T(8,128)}) custom-call(f32[96,1024]{1,0:T(8,128)S(1)} %get-tuple-element.46.own, bf16[96,1024]{1,0:T(8,128)(2,1)S(1)} %collective-permute-done.13.behind, bf16[96,1024]{1,0:T(8,128)(2,1)S(1)} %collective-permute-done.15.ahead, bf16[352,256]{1,0:T(8,128)(2,1)S(1)} %add_convert_fusion.4.down_a, ...), custom_call_target="tpu_custom_call" | custom-call | tf_op jit(solution)/shard_map/pallas_call | solution.py:123
  75.7 0.9 %shard_map.90 = (f32[352,256]{1,0:T(8,128)}, f32[352,256]{1,0:T(8,128)}) custom-call(bf16[704,256]{1,0:T(8,128)(2,1)S(1)} %add_convert_fusion.a, bf16[704,256]{1,0:T(8,128)(2,1)S(1)} %collective-permute-done.25.b), custom_call_target="tpu_custom_call" | custom-call | tf_op jit(solution)/shard_map/pallas_call | solution.py:123
  (18 shorter events, 0.2 us)
Async XLA Ops:
  1.9 3.8 %collective-permute-start.8 = (bf16[1056,256]{1,0:T(8,128)(2,1)S(1)}, bf16[1056,256]{1,0:T(8,128)(2,1)S(1)}, u32[]{:S(2)}, u32[]{:S(2)}) collective-permute-start(bf16[1056,256]{1,0:T(8,128)(2,1)S(1)} %get-tuple-element.34.r_8_), channel_id=1, source_target_pairs={{0,1},{1,0},{2,3},{3,2},{4,5},{5,4},{6,7},{7,6},{8,9},{9,8},{10,11... | collective-permute-start | bytes 1622024 | tf_op jit(solution)/shard_map/ppermute | solution.py:134
  2.0 5.3 %collective-permute-start.2 = (bf16[192,1024]{1,0:T(8,128)(2,1)S(1)}, bf16[192,1024]{1,0:T(8,128)(2,1)S(1)}, u32[]{:S(2)}, u32[]{:S(2)}) collective-permute-start(bf16[192,1024]{1,0:T(8,128)(2,1)S(1)} %get-tuple-element.33.r_0_), channel_id=1, source_target_pairs={{0,1},{1,0},{2,3},{3,2},{4,5},{5,4},{6,7},{7,6},{8,9},{9,8},{10,11... | collective-permute-start | bytes 1179656 | tf_op jit(solution)/shard_map/ppermute | solution.py:134
  2.5 9.0 %collective-permute-start = (bf16[192,1024]{1,0:T(8,128)(2,1)S(1)}, bf16[192,1024]{1,0:T(8,128)(2,1)S(1)}, u32[]{:S(2)}, u32[]{:S(2)}) collective-permute-start(bf16[192,1024]{1,0:T(8,128)(2,1)S(1)} %get-tuple-element.33.r_0_), channel_id=1, source_target_pairs={{0,2},{1,7},{2,4},{3,1},{4,6},{5,3},{6,0},{7,5},{8,10},{9,15},{10,... | collective-permute-start | bytes 1179656 | tf_op jit(solution)/shard_map/ppermute | solution.py:159
  4.1 10.6 %collective-permute-start.7 = (bf16[1056,256]{1,0:T(8,128)(2,1)S(1)}, bf16[1056,256]{1,0:T(8,128)(2,1)S(1)}, u32[]{:S(2)}, u32[]{:S(2)}) collective-permute-start(bf16[1056,256]{1,0:T(8,128)(2,1)S(1)} %get-tuple-element.34.r_8_), channel_id=1, source_target_pairs={{0,8},{1,25},{8,16},{9,1},{16,24},{17,9},{24,0},{25,17},{2,10},{3,... | collective-permute-start | bytes 1622024 | tf_op jit(solution)/shard_map/ppermute | solution.py:158
  5.7 14.8 %collective-permute-start.9 = (bf16[1056,256]{1,0:T(8,128)(2,1)S(1)}, bf16[1056,256]{1,0:T(8,128)(2,1)S(1)}, u32[]{:S(2)}, u32[]{:S(2)}) collective-permute-start(bf16[1056,256]{1,0:T(8,128)(2,1)S(1)} %collective-permute-done.8), channel_id=1, source_target_pairs={{0,8},{1,25},{8,16},{9,1},{16,24},{17,9},{24,0},{25,17},{2,10},{3,... | collective-permute-start | bytes 1622024 | tf_op jit(solution)/shard_map/ppermute | solution.py:161
  7.3 13.7 %collective-permute-start.3 = (bf16[192,1024]{1,0:T(8,128)(2,1)S(1)}, bf16[192,1024]{1,0:T(8,128)(2,1)S(1)}, u32[]{:S(2)}, u32[]{:S(2)}) collective-permute-start(bf16[192,1024]{1,0:T(8,128)(2,1)S(1)} %collective-permute-done.2.r_4_), channel_id=1, source_target_pairs={{0,2},{1,7},{2,4},{3,1},{4,6},{5,3},{6,0},{7,5},{8,10},{9,15},{10,... | collective-permute-start | bytes 1179656 | tf_op jit(solution)/shard_map/ppermute | solution.py:162
  11.5 9.5 %collective-permute-start.1 = (bf16[192,1024]{1,0:T(8,128)(2,1)S(1)}, bf16[192,1024]{1,0:T(8,128)(2,1)S(1)}, u32[]{:S(2)}, u32[]{:S(2)}) collective-permute-start(bf16[192,1024]{1,0:T(8,128)(2,1)S(1)} %collective-permute-done.r_1_), channel_id=1, source_target_pairs={{0,2},{1,7},{2,4},{3,1},{4,6},{5,3},{6,0},{7,5},{8,10},{9,15},{10,... | collective-permute-start | bytes 1179656 | tf_op jit(solution)/shard_map/ppermute | solution.py:164
  14.7 11.6 %collective-permute-start.11 = (bf16[1056,256]{1,0:T(8,128)(2,1)S(1)}, bf16[1056,256]{1,0:T(8,128)(2,1)S(1)}, u32[]{:S(2)}, u32[]{:S(2)}) collective-permute-start(bf16[1056,256]{1,0:T(8,128)(2,1)S(1)} %collective-permute-done.7.r_9_), channel_id=1, source_target_pairs={{0,8},{1,25},{8,16},{9,1},{16,24},{17,9},{24,0},{25,17},{2,10},{3,... | collective-permute-start | bytes 1622024 | tf_op jit(solution)/shard_map/ppermute | solution.py:163
  20.5 5.8 %collective-permute-start.10 = (bf16[1056,256]{1,0:T(8,128)(2,1)S(1)}, bf16[1056,256]{1,0:T(8,128)(2,1)S(1)}, u32[]{:S(2)}, u32[]{:S(2)}) collective-permute-start(bf16[1056,256]{1,0:T(8,128)(2,1)S(1)} %collective-permute-done.9), channel_id=1, source_target_pairs={{0,1},{1,0},{2,3},{3,2},{4,5},{5,4},{6,7},{7,6},{8,9},{9,8},{10,11... | collective-permute-start | bytes 1622024 | tf_op jit(solution)/shard_map/ppermute | solution.py:134
  20.5 2.5 %collective-permute-start.5 = (bf16[192,1024]{1,0:T(8,128)(2,1)S(1)}, bf16[192,1024]{1,0:T(8,128)(2,1)S(1)}, u32[]{:S(2)}, u32[]{:S(2)}) collective-permute-start(bf16[192,1024]{1,0:T(8,128)(2,1)S(1)} %collective-permute-done.r_1_), channel_id=1, source_target_pairs={{0,1},{1,0},{2,3},{3,2},{4,5},{5,4},{6,7},{7,6},{8,9},{9,8},{10,11... | collective-permute-start | bytes 1179656 | tf_op jit(solution)/shard_map/ppermute | solution.py:134
  21.0 5.3 %collective-permute-start.4 = (bf16[192,1024]{1,0:T(8,128)(2,1)S(1)}, bf16[192,1024]{1,0:T(8,128)(2,1)S(1)}, u32[]{:S(2)}, u32[]{:S(2)}) collective-permute-start(bf16[192,1024]{1,0:T(8,128)(2,1)S(1)} %collective-permute-done.3.r_7_), channel_id=1, source_target_pairs={{0,1},{1,0},{2,3},{3,2},{4,5},{5,4},{6,7},{7,6},{8,9},{9,8},{10,11... | collective-permute-start | bytes 1179656 | tf_op jit(solution)/shard_map/ppermute | solution.py:134
  21.0 5.3 %collective-permute-start.6 = (bf16[192,1024]{1,0:T(8,128)(2,1)S(1)}, bf16[192,1024]{1,0:T(8,128)(2,1)S(1)}, u32[]{:S(2)}, u32[]{:S(2)}) collective-permute-start(bf16[192,1024]{1,0:T(8,128)(2,1)S(1)} %collective-permute-done.1.r_2_), channel_id=1, source_target_pairs={{0,1},{1,0},{2,3},{3,2},{4,5},{5,4},{6,7},{7,6},{8,9},{9,8},{10,11... | collective-permute-start | bytes 1179656 | tf_op jit(solution)/shard_map/ppermute | solution.py:134
  31.0 10.8 %collective-permute-start.22 = (bf16[704,256]{1,0:T(8,128)(2,1)S(1)}, bf16[704,256]{1,0:T(8,128)(2,1)S(1)}, u32[]{:S(2)}, u32[]{:S(2)}) collective-permute-start(bf16[704,256]{1,0:T(8,128)(2,1)S(1)} %get-tuple-element.58), channel_id=1, source_target_pairs={{0,8},{1,25},{8,16},{9,1},{16,24},{17,9},{24,0},{25,17},{2,10},{3,... | collective-permute-start | bytes 1081352 | tf_op jit(solution)/shard_map/ppermute | solution.py:181
  31.4 14.1 %collective-permute-start.17 = (bf16[352,256]{1,0:T(8,128)(2,1)S(1)}, bf16[352,256]{1,0:T(8,128)(2,1)S(1)}, u32[]{:S(2)}, u32[]{:S(2)}) collective-permute-start(bf16[352,256]{1,0:T(8,128)(2,1)S(1)} %get-tuple-element.53), channel_id=1, source_target_pairs={{0,8},{1,25},{8,16},{9,1},{16,24},{17,9},{24,0},{25,17},{2,10},{3,... | collective-permute-start | bytes 540680 | tf_op jit(solution)/shard_map/ppermute | solution.py:181
  33.0 12.6 %collective-permute-start.21 = (bf16[704,256]{1,0:T(8,128)(2,1)S(1)}, bf16[704,256]{1,0:T(8,128)(2,1)S(1)}, u32[]{:S(2)}, u32[]{:S(2)}) collective-permute-start(bf16[704,256]{1,0:T(8,128)(2,1)S(1)} %get-tuple-element.56), channel_id=1, source_target_pairs={{8,0},{25,1},{16,8},{1,9},{24,16},{9,17},{0,24},{17,25},{10,2},{27... | collective-permute-start | bytes 1081352 | tf_op jit(solution)/shard_map/ppermute | solution.py:182
  36.5 18.3 %collective-permute-start.12 = (bf16[384,1024]{1,0:T(8,128)(2,1)S(1)}, bf16[384,1024]{1,0:T(8,128)(2,1)S(1)}, u32[]{:S(2)}, u32[]{:S(2)}) collective-permute-start(bf16[384,1024]{1,0:T(8,128)(2,1)S(1)} %get-tuple-element.45), channel_id=1, source_target_pairs={{0,1},{1,0},{2,3},{3,2},{4,5},{5,4},{6,7},{7,6},{8,9},{9,8},{10,11... | collective-permute-start | bytes 2359304 | tf_op jit(solution)/shard_map/ppermute | solution.py:134
  41.9 10.6 %collective-permute-start.23 = (bf16[704,256]{1,0:T(8,128)(2,1)S(1)}, bf16[704,256]{1,0:T(8,128)(2,1)S(1)}, u32[]{:S(2)}, u32[]{:S(2)}) collective-permute-start(bf16[704,256]{1,0:T(8,128)(2,1)S(1)} %add_convert_fusion.2), channel_id=1, source_target_pairs={{0,8},{1,25},{8,16},{9,1},{16,24},{17,9},{24,0},{25,17},{2,10},{3,... | collective-permute-start | bytes 1081352 | tf_op jit(solution)/shard_map/ppermute | solution.py:183
  42.0 14.0 %collective-permute-start.16 = (bf16[352,256]{1,0:T(8,128)(2,1)S(1)}, bf16[352,256]{1,0:T(8,128)(2,1)S(1)}, u32[]{:S(2)}, u32[]{:S(2)}) collective-permute-start(bf16[352,256]{1,0:T(8,128)(2,1)S(1)} %get-tuple-element.51), channel_id=1, source_target_pairs={{8,0},{25,1},{16,8},{1,9},{24,16},{9,17},{0,24},{17,25},{10,2},{27... | collective-permute-start | bytes 540680 | tf_op jit(solution)/shard_map/ppermute | solution.py:182
  45.6 10.4 %collective-permute-start.18 = (bf16[352,256]{1,0:T(8,128)(2,1)S(1)}, bf16[352,256]{1,0:T(8,128)(2,1)S(1)}, u32[]{:S(2)}, u32[]{:S(2)}) collective-permute-start(bf16[352,256]{1,0:T(8,128)(2,1)S(1)} %add_convert_fusion.6), channel_id=1, source_target_pairs={{0,8},{1,25},{8,16},{9,1},{16,24},{17,9},{24,0},{25,17},{2,10},{3,... | collective-permute-start | bytes 540680 | tf_op jit(solution)/shard_map/ppermute | solution.py:183
  52.7 11.4 %collective-permute-start.24 = (bf16[704,256]{1,0:T(8,128)(2,1)S(1)}, bf16[704,256]{1,0:T(8,128)(2,1)S(1)}, u32[]{:S(2)}, u32[]{:S(2)}) collective-permute-start(bf16[704,256]{1,0:T(8,128)(2,1)S(1)} %add_convert_fusion.1), channel_id=1, source_target_pairs={{0,32},{1,97},{32,0},{33,65},{64,96},{65,33},{96,64},{97,1},{2,34}... | collective-permute-start | bytes 1081352 | tf_op jit(solution)/shard_map/ppermute | solution.py:188
  55.0 9.0 %collective-permute-start.14 = (bf16[96,1024]{1,0:T(8,128)(2,1)S(1)}, bf16[96,1024]{1,0:T(8,128)(2,1)S(1)}, u32[]{:S(2)}, u32[]{:S(2)}) collective-permute-start(bf16[96,1024]{1,0:T(8,128)(2,1)S(1)} %get-tuple-element.49), channel_id=1, source_target_pairs={{0,2},{1,7},{2,4},{3,1},{4,6},{5,3},{6,0},{7,5},{8,10},{9,15},{10,... | collective-permute-start | bytes 589832 | tf_op jit(solution)/shard_map/ppermute | solution.py:181
  56.0 10.5 %collective-permute-start.19 = (bf16[352,256]{1,0:T(8,128)(2,1)S(1)}, bf16[352,256]{1,0:T(8,128)(2,1)S(1)}, u32[]{:S(2)}, u32[]{:S(2)}) collective-permute-start(bf16[352,256]{1,0:T(8,128)(2,1)S(1)} %add_convert_fusion.5), channel_id=1, source_target_pairs={{0,32},{1,97},{32,0},{33,65},{64,96},{65,33},{96,64},{97,1},{2,34}... | collective-permute-start | bytes 540680 | tf_op jit(solution)/shard_map/ppermute | solution.py:188
  56.5 18.3 %collective-permute-start.13 = (bf16[96,1024]{1,0:T(8,128)(2,1)S(1)}, bf16[96,1024]{1,0:T(8,128)(2,1)S(1)}, u32[]{:S(2)}, u32[]{:S(2)}) collective-permute-start(bf16[96,1024]{1,0:T(8,128)(2,1)S(1)} %get-tuple-element.47), channel_id=1, source_target_pairs={{2,0},{7,1},{4,2},{1,3},{6,4},{3,5},{0,6},{5,7},{10,8},{15,9},{12,... | collective-permute-start | bytes 589832 | tf_op jit(solution)/shard_map/ppermute | solution.py:182
  64.0 10.8 %collective-permute-start.15 = (bf16[96,1024]{1,0:T(8,128)(2,1)S(1)}, bf16[96,1024]{1,0:T(8,128)(2,1)S(1)}, u32[]{:S(2)}, u32[]{:S(2)}) collective-permute-start(bf16[96,1024]{1,0:T(8,128)(2,1)S(1)} %add_convert_fusion.3), channel_id=1, source_target_pairs={{0,2},{1,7},{2,4},{3,1},{4,6},{5,3},{6,0},{7,5},{8,10},{9,15},{10,... | collective-permute-start | bytes 589832 | tf_op jit(solution)/shard_map/ppermute | solution.py:183
  64.2 11.5 %collective-permute-start.25 = (bf16[704,256]{1,0:T(8,128)(2,1)S(1)}, bf16[704,256]{1,0:T(8,128)(2,1)S(1)}, u32[]{:S(2)}, u32[]{:S(2)}) collective-permute-start(bf16[704,256]{1,0:T(8,128)(2,1)S(1)} %add_convert_fusion.a), channel_id=1, source_target_pairs={{0,96},{1,33},{32,64},{33,1},{64,32},{65,97},{96,0},{97,65},{2,98}... | collective-permute-start | bytes 1081352 | tf_op jit(solution)/shard_map/ppermute | solution.py:189
  66.6 8.3 %collective-permute-start.20 = (bf16[352,256]{1,0:T(8,128)(2,1)S(1)}, bf16[352,256]{1,0:T(8,128)(2,1)S(1)}, u32[]{:S(2)}, u32[]{:S(2)}) collective-permute-start(bf16[352,256]{1,0:T(8,128)(2,1)S(1)} %add_convert_fusion.4.down_a), channel_id=1, source_target_pairs={{0,96},{1,33},{32,64},{33,1},{64,32},{65,97},{96,0},{97,65},{2,98}... | collective-permute-start | bytes 540680 | tf_op jit(solution)/shard_map/ppermute | solution.py:189
where the time goes:
time: 77.1 us; the launch traced here: 76.6 us
  waiting for transfers between devices  40.2 us (52%)
  starting transfers between devices  25.4 us (33%)
  Pallas kernels  9.69 us (13%)
  between operations  0.78 us (1%)
    ppermute x3, waiting for transfers between devices, scattered(): relayed = lax.ppermute(far, axes, UP)  10.4 us
    pallas_call x7, Pallas kernels, call(): pl.pallas_call(kernel, out_shape=[outputs(*o) if outputs else jax.ShapeDt...  9.69 us
    ppermute x2, waiting for transfers between devices, reduced(): return (pair, lax.ppermute(pair, z_axis, CROSS))  7.2 us
    ppermute x3, starting transfers between devices, scattered(): back = lax.ppermute(behind, axes, DOWN)  6.9 us
    ppermute x3, waiting for transfers between devices, scattered(): front = lax.ppermute(plus(ahead, relayed), axes, UP)  6.87 us
    ppermute x1, waiting for transfers between devices, body(): w_second = lax.ppermute(w_other, y_axis, UP)  5.43 us
    ppermute x2, starting transfers between devices, reduced(): return (pair, lax.ppermute(pair, z_axis, CROSS))  3.4 us
    ppermute x1, waiting for transfers between devices, body(): w_far = lax.ppermute(w_behind, y_axis, UP)  3.3 us
  transfers between devices with their start and end apart: 26, of which 10 were waited for; matrix products, arithmetic and copies ran while one was open for 1% of the time, Pallas kernels for 4%

commit v1 on v0

--- a/solution.py
+++ b/solution.py
@@ -37,14 +37,14 @@
     ]
 
 
-def pack_kernel(x, g, wg, wu, wd, xg, w, sems):
+def pack_kernel(x, g, wg, wu, wd, xg, w, d, sems):
     rows, hid = x.shape[0], wg.shape[0]
     places = (
-        (wg, w.at[:hid]),
-        (wu, w.at[hid : 2 * hid]),
-        (wd, w.at[2 * hid :]),
         (x, xg.at[:rows]),
         (g, xg.at[rows:]),
+        (wg, w.at[:hid]),
+        (wu, w.at[hid:]),
+        (wd, d),
     )
     copies = [pltpu.make_async_copy(a, b, sems.at[i]) for i, (a, b) in enumerate(places)]
     for copy in copies:
@@ -55,7 +55,7 @@
 
 def forward_kernel(factor, *refs):
     blocks, weights = refs[:8], refs[8:12]
-    xs, gs, gate_t, up_t, wg, wu, wd, own, behind, ahead, far = refs[12:]
+    xs, gs, gate_t, up_t, wg, wu, own, behind, ahead, far = refs[12:]
     rows = blocks[0].shape[0] // 2
     hid, width = own.shape
     places = columns_of(width)
@@ -64,8 +64,7 @@
         gs[i * rows : (i + 1) * rows] = b[rows:]
     for ref, cols in zip(weights, places):
         wg[:, cols] = ref[:hid]
-        wu[:, cols] = ref[hid : 2 * hid]
-        wd[:, cols] = ref[2 * hid :]
+        wu[:, cols] = ref[hid:]
     gate = nt(wg[...], xs[...]).astype(BF)
     up = nt(wu[...], xs[...]).astype(BF)
     gate_t[...] = gate
@@ -76,8 +75,12 @@
         out[...] = (factor * nn(hidden, gs[:, cols])).astype(BF)
 
 
-def backward_kernel(factor, xs, gs, gate_t, up_t, wd, gg_t, gu_t, *outs):
-    hid = wd.shape[0]
+def backward_kernel(factor, xs, gs, gate_t, up_t, *refs):
+    weights, (gg_t, gu_t), outs, wd = refs[:4], refs[4:6], refs[6:10], refs[10]
+    hid, width = weights[0].shape
+    places = columns_of(width)
+    for ref, cols in zip(weights, places):
+        wd[:, cols] = ref[...]
     grad = nt(wd[...], gs[...]).astype(BF).astype(F32)
     gate = gate_t[...].astype(F32)
     up = up_t[...].astype(F32)
@@ -86,7 +89,7 @@
     grad_up = (grad * (gate * sig)).astype(BF)
     gg_t[...] = grad_gate
     gu_t[...] = grad_up
-    for out, cols in zip(outs, columns_of(outs[0].shape[1])):
+    for out, cols in zip(outs, places):
         x = xs[:, cols]
         out[:hid] = (factor * nn(grad_gate, x)).astype(BF)
         out[hid:] = (factor * nn(grad_up, x)).astype(BF)
@@ -105,15 +108,15 @@
         out[...] = (mine[part] + other[part].astype(F32)).astype(out.dtype)
 
 
-def outputs_kernel(own, behind, ahead, down_a, down_b, grad_in, down):
+def grad_kernel(own, behind, ahead, grad_in):
     grad_in[...] = (own[...] + behind[...].astype(F32) + ahead[...].astype(F32)).astype(BF)
-    down[...] = down_a[...].astype(F32) + down_b[...].astype(F32)
-
-
-def weights_kernel(a, b, gate, up):
+
+
+def weights_kernel(a, b, down_a, down_b, gate, up, down):
     hid = gate.shape[0]
     gate[...] = a[:hid].astype(F32) + b[:hid].astype(F32)
     up[...] = a[hid:].astype(F32) + b[hid:].astype(F32)
+    down[...] = down_a[...].astype(F32) + down_b[...].astype(F32)
 
 
 def call(kernel, outs, *args, inputs=pltpu.VMEM, outputs=pltpu.VMEM, scratch=()):
@@ -144,9 +147,9 @@
     toks = 8 * rows
     factor = (toks * 16) ** (-0.5)
     x_axis, y_axis, z_axis = ("tx", "tc"), ("fs", "tc"), ("rep", "tc")
-    xg, w = call(
+    xg, w, d = call(
         pack_kernel,
-        [((2 * rows, model), BF), ((3 * hid, width), BF)],
+        [((2 * rows, model), BF), ((2 * hid, width), BF), ((hid, width), BF)],
         tokens_in,
         out_grad,
         gate_weight.T,
@@ -155,25 +158,27 @@
         inputs=pltpu.HBM,
         scratch=[pltpu.SemaphoreType.DMA((5,))],
     )
-    w_behind = lax.ppermute(w, y_axis, UP)
-    x_behind = lax.ppermute(xg, x_axis, UP)
-    w_other, x_other = swap(w), swap(xg)
-    w_second = lax.ppermute(w_other, y_axis, UP)
-    x_second = lax.ppermute(x_other, x_axis, UP)
-    w_far = lax.ppermute(w_behind, y_axis, UP)
-    x_far = lax.ppermute(x_behind, x_axis, UP)
-    w_ahead = swap(w_second)
+
+    def gathered(axes, value):
+        behind = lax.ppermute(value, axes, UP)
+        other = swap(value)
+        second = lax.ppermute(other, axes, UP)
+        return other, behind, second, lax.ppermute(behind, axes, UP)
+
+    x_other, x_behind, x_second, x_far = gathered(x_axis, xg)
+    _, w_behind, w_second, w_far = gathered(y_axis, w)
+    _, d_behind, d_second, d_far = gathered(y_axis, d)
     blocks = [xg, x_behind, x_far, swap(x_second), x_other, swap(x_behind), swap(x_far), x_second]
     big = ((toks, model), BF)
     hidden_shape = ((hid, toks), BF)
     weight = ((hid, model), BF)
-    xs, gs, gate_t, up_t, wg, wu, wd, *downs = call(
+    xs, gs, gate_t, up_t, wg, wu, *downs = call(
         lambda *r: forward_kernel(factor, *r),
-        [big, big, hidden_shape, hidden_shape, weight, weight, weight] + [((hid, width), BF)] * 4,
+        [big, big, hidden_shape, hidden_shape, weight, weight] + [((hid, width), BF)] * 4,
         *blocks,
         w,
         w_behind,
-        w_ahead,
+        swap(w_second),
         w_far,
     )
 
@@ -196,7 +201,11 @@
         gs,
         gate_t,
         up_t,
-        wd,
+        d,
+        d_behind,
+        swap(d_second),
+        d_far,
+        scratch=[pltpu.VMEM((hid, model), BF)],
     )
     both = reduced(*scattered(y_axis, *parts))
     half = ((toks // 2, model),)
@@ -206,10 +215,10 @@
         pair_kernel, [(piece, F32)] + [(piece, BF)] * 3, kept, swap(given)
     )
     grad_parts = scattered(x_axis, own, behind, ahead, far)
-    grad_in, grad_down = call(
-        outputs_kernel, [(piece, BF), ((hid, width), F32)], *grad_parts, *down, outputs=None
-    )
-    grad_gate, grad_up = call(weights_kernel, [((hid, width), F32)] * 2, *both, outputs=None)
+    (grad_in,) = call(grad_kernel, [(piece, BF)], *grad_parts, outputs=None)
+    grad_gate, grad_up, grad_down = call(
+        weights_kernel, [((hid, width), F32)] * 3, *both, *down, outputs=None
+    )
     return (grad_in, grad_gate.T, grad_up.T, grad_down)
 
 

time: 77.1 us -> 84.6 us (1.097)
  starting transfers between devices: 25.4 us -> 35.1 us
  waiting for transfers between devices: 40.2 us -> 38.5 us
    ppermute x6 -> x9, waiting for transfers between devices: 14.2 us -> 22.9 us  [the longest x3 11.4 us: gathered(): return (other, behind, second, lax.ppermute(behind, axes, UP))]
    ppermute x2, starting transfers between devices: 3.4 us -> 9.01 us  [reduced(): return (pair, lax.ppermute(pair, z_axis, CROSS))]
    ppermute x2, waiting for transfers between devices: 7.2 us -> 2.78 us  [reduced(): return (pair, lax.ppermute(pair, z_axis, CROSS))]
    ppermute x6 -> x9, starting transfers between devices: 7.01 us -> 9.71 us  [the longest x3 4.82 us: gathered(): behind = lax.ppermute(value, axes, UP)]
    ppermute x3, waiting for transfers between devices: 6.87 us -> 4.37 us  [scattered(): front = lax.ppermute(plus(ahead, relayed), axes, UP)]
    ppermute x3, waiting for transfers between devices: 10.4 us -> 8.38 us  [scattered(): relayed = lax.ppermute(far, axes, UP)]
    ppermute x3, starting transfers between devices: 2.99 us -> 1.01 us  [scattered(): relayed = lax.ppermute(far, axes, UP)]
    ppermute x3, starting transfers between devices: 0.22 us -> 1.83 us  [scattered(): front = lax.ppermute(plus(ahead, relayed), axes, UP)]
  transfers between devices with their start and end apart: 26 -> 31, of which waited for: 10 -> 8; matrix products, arithmetic and copies ran while one was open for 1% -> 1% of each run, Pallas kernels for 4% -> 6%
where the time goes in v1:
time: 84.6 us; the launch traced here: 84.5 us
  waiting for transfers between devices  38.5 us (46%)
  starting transfers between devices  35.1 us (41%)
  Pallas kernels  9.64 us (11%)
    ppermute x3, waiting for transfers between devices, gathered(): return (other, behind, second, lax.ppermute(behind, axes, UP))  11.4 us
    pallas_call x7, Pallas kernels, call(): pl.pallas_call(kernel, out_shape=[outputs(*o) if outputs else jax.ShapeDt...  9.64 us
    ppermute x2, starting transfers between devices, reduced(): return (pair, lax.ppermute(pair, z_axis, CROSS))  9.01 us
    ppermute x3, waiting for transfers between devices, scattered(): relayed = lax.ppermute(far, axes, UP)  8.38 us
    ppermute x3, waiting for transfers between devices, gathered(): second = lax.ppermute(other, axes, UP)  8.03 us
    ppermute x3, starting transfers between devices, scattered(): back = lax.ppermute(behind, axes, DOWN)  7.79 us
    ppermute x3, starting transfers between devices, gathered(): behind = lax.ppermute(value, axes, UP)  4.82 us
    ppermute x3, waiting for transfers between devices, scattered(): front = lax.ppermute(plus(ahead, relayed), axes, UP)  4.37 us
  transfers between devices with their start and end apart: 31, of which 8 were waited for; matrix products, arithmetic and copies ran while one was open for 1% of the time, Pallas kernels for 6%

profile of v1, /device:TPU:0, one launch (start us, length us, event | category | flops | bytes accessed | tf_op | source)
XLA Modules:
  0.0 84.5 jit_solution(7523086605686155714)
XLA Ops:
  0.6 1.3 %shard_map.84 = (bf16[192,1024]{1,0:T(8,128)(2,1)S(1)}, bf16[704,256]{1,0:T(8,128)(2,1)S(1)}, bf16[352,256]{1,0:T(8,128)(2,1)S(1)}) custom-call(bf16[96,1024]{1,0:T(8,128)(2,1)} %x.1, bf16[96,1024]{1,0:T(8,128)(2,1)} %g.1, bf16[352,256]{1,0:T(8,128)(2,1)} %bitcast.4, bf16[352,256]{1,0:T(8,128)(2,1)} %bitcast.5, bf16[352,256]{1,0:T(8,128)(2,1)} %wd.1), custom_call_target="tpu_custom_call" | custom-call | tf_op jit(solution)/shard_map/pallas_call | solution.py:126
  1.9 1.7 %collective-permute-start = (bf16[192,1024]{1,0:T(8,128)(2,1)S(1)}, bf16[192,1024]{1,0:T(8,128)(2,1)S(1)}, u32[]{:S(2)}, u32[]{:S(2)}) collective-permute-start(bf16[192,1024]{1,0:T(8,128)(2,1)S(1)} %get-tuple-element.32.r_0_), channel_id=1, source_target_pairs={{0,2},{1,7},{2,4},{3,1},{4,6},{5,3},{6,0},{7,5},{8,10},{9,15},{10,... | collective-permute-start | bytes 1179656 | tf_op jit(solution)/shard_map/ppermute | solution.py:163
  3.6 0.8 collective-permute-start.2
  4.4 1.6 %collective-permute-start.12 = (bf16[352,256]{1,0:T(8,128)(2,1)S(1)}, bf16[352,256]{1,0:T(8,128)(2,1)S(1)}, u32[]{:S(2)}, u32[]{:S(2)}) collective-permute-start(bf16[352,256]{1,0:T(8,128)(2,1)S(1)} %get-tuple-element.38.r_4_), channel_id=1, source_target_pairs={{0,8},{1,25},{8,16},{9,1},{16,24},{17,9},{24,0},{25,17},{2,10},{3,... | collective-permute-start | bytes 540680 | tf_op jit(solution)/shard_map/ppermute | solution.py:163
  6.0 1.6 %collective-permute-start.7 = (bf16[704,256]{1,0:T(8,128)(2,1)S(1)}, bf16[704,256]{1,0:T(8,128)(2,1)S(1)}, u32[]{:S(2)}, u32[]{:S(2)}) collective-permute-start(bf16[704,256]{1,0:T(8,128)(2,1)S(1)} %get-tuple-element.33.r_8_), channel_id=1, source_target_pairs={{0,8},{1,25},{8,16},{9,1},{16,24},{17,9},{24,0},{25,17},{2,10},{3,... | collective-permute-start | bytes 1081352 | tf_op jit(solution)/shard_map/ppermute | solution.py:163
  7.6 3.6 %collective-permute-done.12.r_5_ = bf16[352,256]{1,0:T(8,128)(2,1)S(1)} collective-permute-done((bf16[352,256]{1,0:T(8,128)(2,1)S(1)}, bf16[352,256]{1,0:T(8,128)(2,1)S(1)}, u32[]{:S(2)}, u32[]{:S(2)}) %collective-permute-start.12) | collective-permute-done | bytes 180256 | tf_op jit(solution)/shard_map/ppermute | solution.py:163
  11.1 0.0 collective-permute-start.13
  11.2 0.0 collective-permute-done.r_1_
  11.2 1.2 %collective-permute-start.1 = (bf16[192,1024]{1,0:T(8,128)(2,1)S(1)}, bf16[192,1024]{1,0:T(8,128)(2,1)S(1)}, u32[]{:S(2)}, u32[]{:S(2)}) collective-permute-start(bf16[192,1024]{1,0:T(8,128)(2,1)S(1)} %collective-permute-done.r_1_), channel_id=1, source_target_pairs={{0,2},{1,7},{2,4},{3,1},{4,6},{5,3},{6,0},{7,5},{8,10},{9,15},{10,... | collective-permute-start | bytes 1179656 | tf_op jit(solution)/shard_map/ppermute | solution.py:166
  12.3 1.2 %collective-permute-start.3 = (bf16[192,1024]{1,0:T(8,128)(2,1)S(1)}, bf16[192,1024]{1,0:T(8,128)(2,1)S(1)}, u32[]{:S(2)}, u32[]{:S(2)}) collective-permute-start(bf16[192,1024]{1,0:T(8,128)(2,1)S(1)} %collective-permute-done.2.r_4_), channel_id=1, source_target_pairs={{0,2},{1,7},{2,4},{3,1},{4,6},{5,3},{6,0},{7,5},{8,10},{9,15},{10,... | collective-permute-start | bytes 1179656 | tf_op jit(solution)/shard_map/ppermute | solution.py:165
  13.5 0.9 %collective-permute-start.9 = (bf16[704,256]{1,0:T(8,128)(2,1)S(1)}, bf16[704,256]{1,0:T(8,128)(2,1)S(1)}, u32[]{:S(2)}, u32[]{:S(2)}) collective-permute-start(bf16[704,256]{1,0:T(8,128)(2,1)S(1)} %collective-permute-done.8), channel_id=1, source_target_pairs={{0,8},{1,25},{8,16},{9,1},{16,24},{17,9},{24,0},{25,17},{2,10},{3,... | collective-permute-start | bytes 1081352 | tf_op jit(solution)/shard_map/ppermute | solution.py:165
  14.5 1.6 %collective-permute-start.14 = (bf16[352,256]{1,0:T(8,128)(2,1)S(1)}, bf16[352,256]{1,0:T(8,128)(2,1)S(1)}, u32[]{:S(2)}, u32[]{:S(2)}) collective-permute-start(bf16[352,256]{1,0:T(8,128)(2,1)S(1)} %collective-permute-done.13), channel_id=1, source_target_pairs={{0,8},{1,25},{8,16},{9,1},{16,24},{17,9},{24,0},{25,17},{2,10},{3,... | collective-permute-start | bytes 540680 | tf_op jit(solution)/shard_map/ppermute | solution.py:165
  16.1 0.0 collective-permute-start.5
  16.1 8.0 %collective-permute-done.14 = bf16[352,256]{1,0:T(8,128)(2,1)S(1)} collective-permute-done((bf16[352,256]{1,0:T(8,128)(2,1)S(1)}, bf16[352,256]{1,0:T(8,128)(2,1)S(1)}, u32[]{:S(2)}, u32[]{:S(2)}) %collective-permute-start.14) | collective-permute-done | bytes 180256 | tf_op jit(solution)/shard_map/ppermute | solution.py:165
  24.1 1.2 %collective-permute-start.6 = (bf16[192,1024]{1,0:T(8,128)(2,1)S(1)}, bf16[192,1024]{1,0:T(8,128)(2,1)S(1)}, u32[]{:S(2)}, u32[]{:S(2)}) collective-permute-start(bf16[192,1024]{1,0:T(8,128)(2,1)S(1)} %collective-permute-done.1.r_2_), channel_id=1, source_target_pairs={{0,1},{1,0},{2,3},{3,2},{4,5},{5,4},{6,7},{7,6},{8,9},{9,8},{10,11... | collective-permute-start | bytes 1179656 | tf_op jit(solution)/shard_map/ppermute | solution.py:137
  25.3 0.1 collective-permute-start.4
  25.4 0.4 collective-permute-start.10
  25.8 6.9 %collective-permute-done.11.r_11_ = bf16[704,256]{1,0:T(8,128)(2,1)S(1)} collective-permute-done((bf16[704,256]{1,0:T(8,128)(2,1)S(1)}, bf16[704,256]{1,0:T(8,128)(2,1)S(1)}, u32[]{:S(2)}, u32[]{:S(2)}) %collective-permute-start.11) | collective-permute-done | bytes 360480 | tf_op jit(solution)/shard_map/ppermute | solution.py:166
  32.7 0.1 collective-permute-start.15
  32.8 2.1 %shard_map.85 = (bf16[768,1024]{1,0:T(8,128)(2,1)S(1)}, bf16[768,1024]{1,0:T(8,128)(2,1)S(1)}, bf16[352,768]{1,0:T(8,128)(2,1)S(1)}, bf16[352,768]{1,0:T(8,128)(...) custom-call(bf16[192,1024]{1,0:T(8,128)(2,1)S(1)} %get-tuple-element, ...), custom_call_target="tpu_custom_call" | custom-call | tf_op jit(solution)/shard_map/pallas_call | solution.py:126
  35.0 4.5 %collective-permute-done.16.r_7_ = bf16[352,256]{1,0:T(8,128)(2,1)S(1)} collective-permute-done((bf16[352,256]{1,0:T(8,128)(2,1)S(1)}, bf16[352,256]{1,0:T(8,128)(2,1)S(1)}, u32[]{:S(2)}, u32[]{:S(2)}) %collective-permute-start.16) | collective-permute-done | bytes 180256 | tf_op jit(solution)/shard_map/ppermute | solution.py:166
  39.5 2.5 %shard_map.86 = (bf16[352,768]{1,0:T(8,128)(2,1)S(1)}, bf16[352,768]{1,0:T(8,128)(2,1)S(1)}, bf16[704,256]{1,0:T(8,128)(2,1)S(1)}, bf16[704,256]{1,0:T(8,128)(2,...) custom-call(bf16[768,1024]{1,0:T(8,128)(2,1)S(1)} %get-tuple-element.34.r_0_, ...), custom_call_target="tpu_custom_call" | custom-call | tf_op jit(solution)/shard_map/pallas_call | solution.py:126
  42.0 0.1 collective-permute-start.22
  42.0 0.1 collective-permute-start.27
  42.1 3.2 %collective-permute-start.21 = (bf16[704,256]{1,0:T(8,128)(2,1)S(1)}, bf16[704,256]{1,0:T(8,128)(2,1)S(1)}, u32[]{:S(2)}, u32[]{:S(2)}) collective-permute-start(bf16[704,256]{1,0:T(8,128)(2,1)S(1)} %get-tuple-element.50), channel_id=1, source_target_pairs={{8,0},{25,1},{16,8},{1,9},{24,16},{9,17},{0,24},{17,25},{10,2},{27... | collective-permute-start | bytes 1081352 | tf_op jit(solution)/shard_map/ppermute | solution.py:187
  45.3 1.8 %shard_map.87 = (f32[384,1024]{1,0:T(8,128)S(1)}, bf16[384,1024]{1,0:T(8,128)(2,1)S(1)}) custom-call(bf16[352,768]{1,0:T(8,128)(2,1)S(1)} %get-tuple-element.39.gg_t, bf16[352,768]{1,0:T(8,128)(2,1)S(1)} %get-tuple-element.40.gu_t, bf16[352,1024]{1,0:T(8,128)(2,1)S(1)} %get-tuple-element.41.wg, bf16[352,1024]{1,0:T(8,128)(2,1)S(1)} %get-tuple-element.42.wu), custom_call_target="tpu_custom_call" | custom-call | tf_op jit(solution)/shard_map/pallas_call | solution.py:126
  47.2 0.3 collective-permute-start.17
  47.4 5.2 %collective-permute-done.22 = bf16[704,256]{1,0:T(8,128)(2,1)S(1)} collective-permute-done((bf16[704,256]{1,0:T(8,128)(2,1)S(1)}, bf16[704,256]{1,0:T(8,128)(2,1)S(1)}, u32[]{:S(2)}, u32[]{:S(2)}) %collective-permute-start.22) | collective-permute-done | bytes 360480 | tf_op jit(solution)/shard_map/ppermute | solution.py:186
  52.6 0.1 add_convert_fusion.2
  52.7 0.8 collective-permute-start.23
  53.5 2.5 %collective-permute-start.26 = (bf16[352,256]{1,0:T(8,128)(2,1)S(1)}, bf16[352,256]{1,0:T(8,128)(2,1)S(1)}, u32[]{:S(2)}, u32[]{:S(2)}) collective-permute-start(bf16[352,256]{1,0:T(8,128)(2,1)S(1)} %get-tuple-element.54), channel_id=1, source_target_pairs={{8,0},{25,1},{16,8},{1,9},{24,16},{9,17},{0,24},{17,25},{10,2},{27... | collective-permute-start | bytes 540680 | tf_op jit(solution)/shard_map/ppermute | solution.py:187
  56.1 1.0 %collective-permute-start.28 = (bf16[352,256]{1,0:T(8,128)(2,1)S(1)}, bf16[352,256]{1,0:T(8,128)(2,1)S(1)}, u32[]{:S(2)}, u32[]{:S(2)}) collective-permute-start(bf16[352,256]{1,0:T(8,128)(2,1)S(1)} %add_convert_fusion.6), channel_id=1, source_target_pairs={{0,8},{1,25},{8,16},{9,1},{16,24},{17,9},{24,0},{25,17},{2,10},{3,... | collective-permute-start | bytes 540680 | tf_op jit(solution)/shard_map/ppermute | solution.py:188
  57.1 4.4 %collective-permute-done.23 = bf16[704,256]{1,0:T(8,128)(2,1)S(1)} collective-permute-done((bf16[704,256]{1,0:T(8,128)(2,1)S(1)}, bf16[704,256]{1,0:T(8,128)(2,1)S(1)}, u32[]{:S(2)}, u32[]{:S(2)}) %collective-permute-start.23) | collective-permute-done | bytes 360480 | tf_op jit(solution)/shard_map/ppermute | solution.py:188
  61.4 0.1 add_convert_fusion.1
  61.5 2.0 %collective-permute-start.24 = (bf16[704,256]{1,0:T(8,128)(2,1)S(1)}, bf16[704,256]{1,0:T(8,128)(2,1)S(1)}, u32[]{:S(2)}, u32[]{:S(2)}) collective-permute-start(bf16[704,256]{1,0:T(8,128)(2,1)S(1)} %add_convert_fusion.1), channel_id=1, source_target_pairs={{0,32},{1,97},{32,0},{33,65},{64,96},{65,33},{96,64},{97,1},{2,34}... | collective-permute-start | bytes 1081352 | tf_op jit(solution)/shard_map/ppermute | solution.py:193
  63.6 0.1 shard_map.88
  63.7 0.9 %collective-permute-start.19 = (bf16[96,1024]{1,0:T(8,128)(2,1)S(1)}, bf16[96,1024]{1,0:T(8,128)(2,1)S(1)}, u32[]{:S(2)}, u32[]{:S(2)}) collective-permute-start(bf16[96,1024]{1,0:T(8,128)(2,1)S(1)} %get-tuple-element.48), channel_id=1, source_target_pairs={{0,2},{1,7},{2,4},{3,1},{4,6},{5,3},{6,0},{7,5},{8,10},{9,15},{10,... | collective-permute-start | bytes 589832 | tf_op jit(solution)/shard_map/ppermute | solution.py:186
  64.6 0.1 add_convert_fusion.5
  64.6 0.8 collective-permute-start.29
  65.4 2.0 %collective-permute-start.18 = (bf16[96,1024]{1,0:T(8,128)(2,1)S(1)}, bf16[96,1024]{1,0:T(8,128)(2,1)S(1)}, u32[]{:S(2)}, u32[]{:S(2)}) collective-permute-start(bf16[96,1024]{1,0:T(8,128)(2,1)S(1)} %get-tuple-element.46), channel_id=1, source_target_pairs={{2,0},{7,1},{4,2},{1,3},{6,4},{3,5},{0,6},{5,7},{10,8},{15,9},{12,... | collective-permute-start | bytes 589832 | tf_op jit(solution)/shard_map/ppermute | solution.py:187
  67.5 3.2 %collective-permute-done.19 = bf16[96,1024]{1,0:T(8,128)(2,1)S(1)} collective-permute-done((bf16[96,1024]{1,0:T(8,128)(2,1)S(1)}, bf16[96,1024]{1,0:T(8,128)(2,1)S(1)}, u32[]{:S(2)}, u32[]{:S(2)}) %collective-permute-start.19) | collective-permute-done | bytes 196640 | tf_op jit(solution)/shard_map/ppermute | solution.py:186
  70.7 0.1 collective-permute-start.20
  70.8 0.1 add_convert_fusion.a
  70.9 5.2 %collective-permute-start.25 = (bf16[704,256]{1,0:T(8,128)(2,1)S(1)}, bf16[704,256]{1,0:T(8,128)(2,1)S(1)}, u32[]{:S(2)}, u32[]{:S(2)}) collective-permute-start(bf16[704,256]{1,0:T(8,128)(2,1)S(1)} %add_convert_fusion.a), channel_id=1, source_target_pairs={{0,96},{1,33},{32,64},{33,1},{64,32},{65,97},{96,0},{97,65},{2,98}... | collective-permute-start | bytes 1081352 | tf_op jit(solution)/shard_map/ppermute | solution.py:194
  76.2 3.8 %collective-permute-start.30 = (bf16[352,256]{1,0:T(8,128)(2,1)S(1)}, bf16[352,256]{1,0:T(8,128)(2,1)S(1)}, u32[]{:S(2)}, u32[]{:S(2)}) collective-permute-start(bf16[352,256]{1,0:T(8,128)(2,1)S(1)} %add_convert_fusion.4.down_a), channel_id=1, source_target_pairs={{0,96},{1,33},{32,64},{33,1},{64,32},{65,97},{96,0},{97,65},{2,98}... | collective-permute-start | bytes 540680 | tf_op jit(solution)/shard_map/ppermute | solution.py:194
  80.0 0.7 shard_map.89
  80.7 2.8 %collective-permute-done.30.down_b = bf16[352,256]{1,0:T(8,128)(2,1)S(1)} collective-permute-done((bf16[352,256]{1,0:T(8,128)(2,1)S(1)}, bf16[352,256]{1,0:T(8,128)(2,1)S(1)}, u32[]{:S(2)}, u32[]{:S(2)}) %collective-permute-start.30) | collective-permute-done | bytes 180256 | tf_op jit(solution)/shard_map/ppermute | solution.py:194
  83.5 1.0 %shard_map.90 = (f32[352,256]{1,0:T(8,128)}, f32[352,256]{1,0:T(8,128)}, f32[352,256]{1,0:T(8,128)}) custom-call(bf16[704,256]{1,0:T(8,128)(2,1)S(1)} %add_convert_fusion.a, bf16[704,256]{1,0:T(8,128)(2,1)S(1)} %collective-permute-done.25.b, bf16[352,256]{1,0:T(8,128)(2,1)S(1)} %add_convert_fusion.4.down_a, bf16[352,256]{1,0:T(8,128)(2,1)S(1)} %collective-permute-done.30.down_b), custom_call_target="tpu_custom_call" | custom-call | tf_op jit(solution)/shard_map/pallas_call | solution.py:126
  (28 shorter events, 0.2 us)
Async XLA Ops:
  1.9 9.2 %collective-permute-start = (bf16[192,1024]{1,0:T(8,128)(2,1)S(1)}, bf16[192,1024]{1,0:T(8,128)(2,1)S(1)}, u32[]{:S(2)}, u32[]{:S(2)}) collective-permute-start(bf16[192,1024]{1,0:T(8,128)(2,1)S(1)} %get-tuple-element.32.r_0_), channel_id=1, source_target_pairs={{0,2},{1,7},{2,4},{3,1},{4,6},{5,3},{6,0},{7,5},{8,10},{9,15},{10,... | collective-permute-start | bytes 1179656 | tf_op jit(solution)/shard_map/ppermute | solution.py:163
  3.6 8.7 %collective-permute-start.2 = (bf16[192,1024]{1,0:T(8,128)(2,1)S(1)}, bf16[192,1024]{1,0:T(8,128)(2,1)S(1)}, u32[]{:S(2)}, u32[]{:S(2)}) collective-permute-start(bf16[192,1024]{1,0:T(8,128)(2,1)S(1)} %get-tuple-element.32.r_0_), channel_id=1, source_target_pairs={{0,1},{1,0},{2,3},{3,2},{4,5},{5,4},{6,7},{7,6},{8,9},{9,8},{10,11... | collective-permute-start | bytes 1179656 | tf_op jit(solution)/shard_map/ppermute | solution.py:137
  4.4 9.1 %collective-permute-start.8 = (bf16[704,256]{1,0:T(8,128)(2,1)S(1)}, bf16[704,256]{1,0:T(8,128)(2,1)S(1)}, u32[]{:S(2)}, u32[]{:S(2)}) collective-permute-start(bf16[704,256]{1,0:T(8,128)(2,1)S(1)} %get-tuple-element.33.r_8_), channel_id=1, source_target_pairs={{0,1},{1,0},{2,3},{3,2},{4,5},{5,4},{6,7},{7,6},{8,9},{9,8},{10,11... | collective-permute-start | bytes 1081352 | tf_op jit(solution)/shard_map/ppermute | solution.py:137
  4.4 6.7 %collective-permute-start.12 = (bf16[352,256]{1,0:T(8,128)(2,1)S(1)}, bf16[352,256]{1,0:T(8,128)(2,1)S(1)}, u32[]{:S(2)}, u32[]{:S(2)}) collective-permute-start(bf16[352,256]{1,0:T(8,128)(2,1)S(1)} %get-tuple-element.38.r_4_), channel_id=1, source_target_pairs={{0,8},{1,25},{8,16},{9,1},{16,24},{17,9},{24,0},{25,17},{2,10},{3,... | collective-permute-start | bytes 540680 | tf_op jit(solution)/shard_map/ppermute | solution.py:163
  6.0 10.0 %collective-permute-start.7 = (bf16[704,256]{1,0:T(8,128)(2,1)S(1)}, bf16[704,256]{1,0:T(8,128)(2,1)S(1)}, u32[]{:S(2)}, u32[]{:S(2)}) collective-permute-start(bf16[704,256]{1,0:T(8,128)(2,1)S(1)} %get-tuple-element.33.r_8_), channel_id=1, source_target_pairs={{0,8},{1,25},{8,16},{9,1},{16,24},{17,9},{24,0},{25,17},{2,10},{3,... | collective-permute-start | bytes 1081352 | tf_op jit(solution)/shard_map/ppermute | solution.py:163
  11.1 3.3 %collective-permute-start.13 = (bf16[352,256]{1,0:T(8,128)(2,1)S(1)}, bf16[352,256]{1,0:T(8,128)(2,1)S(1)}, u32[]{:S(2)}, u32[]{:S(2)}) collective-permute-start(bf16[352,256]{1,0:T(8,128)(2,1)S(1)} %get-tuple-element.38.r_4_), channel_id=1, source_target_pairs={{0,1},{1,0},{2,3},{3,2},{4,5},{5,4},{6,7},{7,6},{8,9},{9,8},{10,11... | collective-permute-start | bytes 540680 | tf_op jit(solution)/shard_map/ppermute | solution.py:137
  11.2 13.0 %collective-permute-start.1 = (bf16[192,1024]{1,0:T(8,128)(2,1)S(1)}, bf16[192,1024]{1,0:T(8,128)(2,1)S(1)}, u32[]{:S(2)}, u32[]{:S(2)}) collective-permute-start(bf16[192,1024]{1,0:T(8,128)(2,1)S(1)} %collective-permute-done.r_1_), channel_id=1, source_target_pairs={{0,2},{1,7},{2,4},{3,1},{4,6},{5,3},{6,0},{7,5},{8,10},{9,15},{10,... | collective-permute-start | bytes 1179656 | tf_op jit(solution)/shard_map/ppermute | solution.py:166
  12.3 13.0 %collective-permute-start.3 = (bf16[192,1024]{1,0:T(8,128)(2,1)S(1)}, bf16[192,1024]{1,0:T(8,128)(2,1)S(1)}, u32[]{:S(2)}, u32[]{:S(2)}) collective-permute-start(bf16[192,1024]{1,0:T(8,128)(2,1)S(1)} %collective-permute-done.2.r_4_), channel_id=1, source_target_pairs={{0,2},{1,7},{2,4},{3,1},{4,6},{5,3},{6,0},{7,5},{8,10},{9,15},{10,... | collective-permute-start | bytes 1179656 | tf_op jit(solution)/shard_map/ppermute | solution.py:165
  13.5 11.9 %collective-permute-start.9 = (bf16[704,256]{1,0:T(8,128)(2,1)S(1)}, bf16[704,256]{1,0:T(8,128)(2,1)S(1)}, u32[]{:S(2)}, u32[]{:S(2)}) collective-permute-start(bf16[704,256]{1,0:T(8,128)(2,1)S(1)} %collective-permute-done.8), channel_id=1, source_target_pairs={{0,8},{1,25},{8,16},{9,1},{16,24},{17,9},{24,0},{25,17},{2,10},{3,... | collective-permute-start | bytes 1081352 | tf_op jit(solution)/shard_map/ppermute | solution.py:165
  14.5 9.6 %collective-permute-start.14 = (bf16[352,256]{1,0:T(8,128)(2,1)S(1)}, bf16[352,256]{1,0:T(8,128)(2,1)S(1)}, u32[]{:S(2)}, u32[]{:S(2)}) collective-permute-start(bf16[352,256]{1,0:T(8,128)(2,1)S(1)} %collective-permute-done.13), channel_id=1, source_target_pairs={{0,8},{1,25},{8,16},{9,1},{16,24},{17,9},{24,0},{25,17},{2,10},{3,... | collective-permute-start | bytes 540680 | tf_op jit(solution)/shard_map/ppermute | solution.py:165
  16.1 16.7 %collective-permute-start.5 = (bf16[192,1024]{1,0:T(8,128)(2,1)S(1)}, bf16[192,1024]{1,0:T(8,128)(2,1)S(1)}, u32[]{:S(2)}, u32[]{:S(2)}) collective-permute-start(bf16[192,1024]{1,0:T(8,128)(2,1)S(1)} %collective-permute-done.r_1_), channel_id=1, source_target_pairs={{0,1},{1,0},{2,3},{3,2},{4,5},{5,4},{6,7},{7,6},{8,9},{9,8},{10,11... | collective-permute-start | bytes 1179656 | tf_op jit(solution)/shard_map/ppermute | solution.py:137
  24.1 8.6 %collective-permute-start.11 = (bf16[704,256]{1,0:T(8,128)(2,1)S(1)}, bf16[704,256]{1,0:T(8,128)(2,1)S(1)}, u32[]{:S(2)}, u32[]{:S(2)}) collective-permute-start(bf16[704,256]{1,0:T(8,128)(2,1)S(1)} %collective-permute-done.7.r_9_), channel_id=1, source_target_pairs={{0,8},{1,25},{8,16},{9,1},{16,24},{17,9},{24,0},{25,17},{2,10},{3,... | collective-permute-start | bytes 1081352 | tf_op jit(solution)/shard_map/ppermute | solution.py:166
  24.1 8.7 %collective-permute-start.6 = (bf16[192,1024]{1,0:T(8,128)(2,1)S(1)}, bf16[192,1024]{1,0:T(8,128)(2,1)S(1)}, u32[]{:S(2)}, u32[]{:S(2)}) collective-permute-start(bf16[192,1024]{1,0:T(8,128)(2,1)S(1)} %collective-permute-done.1.r_2_), channel_id=1, source_target_pairs={{0,1},{1,0},{2,3},{3,2},{4,5},{5,4},{6,7},{7,6},{8,9},{9,8},{10,11... | collective-permute-start | bytes 1179656 | tf_op jit(solution)/shard_map/ppermute | solution.py:137
  25.3 7.5 %collective-permute-start.4 = (bf16[192,1024]{1,0:T(8,128)(2,1)S(1)}, bf16[192,1024]{1,0:T(8,128)(2,1)S(1)}, u32[]{:S(2)}, u32[]{:S(2)}) collective-permute-start(bf16[192,1024]{1,0:T(8,128)(2,1)S(1)} %collective-permute-done.3.r_7_), channel_id=1, source_target_pairs={{0,1},{1,0},{2,3},{3,2},{4,5},{5,4},{6,7},{7,6},{8,9},{9,8},{10,11... | collective-permute-start | bytes 1179656 | tf_op jit(solution)/shard_map/ppermute | solution.py:137
  25.4 7.4 %collective-permute-start.10 = (bf16[704,256]{1,0:T(8,128)(2,1)S(1)}, bf16[704,256]{1,0:T(8,128)(2,1)S(1)}, u32[]{:S(2)}, u32[]{:S(2)}) collective-permute-start(bf16[704,256]{1,0:T(8,128)(2,1)S(1)} %collective-permute-done.9), channel_id=1, source_target_pairs={{0,1},{1,0},{2,3},{3,2},{4,5},{5,4},{6,7},{7,6},{8,9},{9,8},{10,11... | collective-permute-start | bytes 1081352 | tf_op jit(solution)/shard_map/ppermute | solution.py:137
  32.7 6.7 %collective-permute-start.16 = (bf16[352,256]{1,0:T(8,128)(2,1)S(1)}, bf16[352,256]{1,0:T(8,128)(2,1)S(1)}, u32[]{:S(2)}, u32[]{:S(2)}) collective-permute-start(bf16[352,256]{1,0:T(8,128)(2,1)S(1)} %collective-permute-done.12.r_5_), channel_id=1, source_target_pairs={{0,8},{1,25},{8,16},{9,1},{16,24},{17,9},{24,0},{25,17},{2,10},{3,... | collective-permute-start | bytes 540680 | tf_op jit(solution)/shard_map/ppermute | solution.py:166
  32.7 6.7 %collective-permute-start.15 = (bf16[352,256]{1,0:T(8,128)(2,1)S(1)}, bf16[352,256]{1,0:T(8,128)(2,1)S(1)}, u32[]{:S(2)}, u32[]{:S(2)}) collective-permute-start(bf16[352,256]{1,0:T(8,128)(2,1)S(1)} %collective-permute-done.14), channel_id=1, source_target_pairs={{0,1},{1,0},{2,3},{3,2},{4,5},{5,4},{6,7},{7,6},{8,9},{9,8},{10,11... | collective-permute-start | bytes 540680 | tf_op jit(solution)/shard_map/ppermute | solution.py:137
  42.0 10.7 %collective-permute-start.22 = (bf16[704,256]{1,0:T(8,128)(2,1)S(1)}, bf16[704,256]{1,0:T(8,128)(2,1)S(1)}, u32[]{:S(2)}, u32[]{:S(2)}) collective-permute-start(bf16[704,256]{1,0:T(8,128)(2,1)S(1)} %get-tuple-element.52), channel_id=1, source_target_pairs={{0,8},{1,25},{8,16},{9,1},{16,24},{17,9},{24,0},{25,17},{2,10},{3,... | collective-permute-start | bytes 1081352 | tf_op jit(solution)/shard_map/ppermute | solution.py:186
  42.0 14.0 %collective-permute-start.27 = (bf16[352,256]{1,0:T(8,128)(2,1)S(1)}, bf16[352,256]{1,0:T(8,128)(2,1)S(1)}, u32[]{:S(2)}, u32[]{:S(2)}) collective-permute-start(bf16[352,256]{1,0:T(8,128)(2,1)S(1)} %get-tuple-element.56), channel_id=1, source_target_pairs={{0,8},{1,25},{8,16},{9,1},{16,24},{17,9},{24,0},{25,17},{2,10},{3,... | collective-permute-start | bytes 540680 | tf_op jit(solution)/shard_map/ppermute | solution.py:186
  42.1 14.9 %collective-permute-start.21 = (bf16[704,256]{1,0:T(8,128)(2,1)S(1)}, bf16[704,256]{1,0:T(8,128)(2,1)S(1)}, u32[]{:S(2)}, u32[]{:S(2)}) collective-permute-start(bf16[704,256]{1,0:T(8,128)(2,1)S(1)} %get-tuple-element.50), channel_id=1, source_target_pairs={{8,0},{25,1},{16,8},{1,9},{24,16},{9,17},{0,24},{17,25},{10,2},{27... | collective-permute-start | bytes 1081352 | tf_op jit(solution)/shard_map/ppermute | solution.py:187
  47.2 16.4 %collective-permute-start.17 = (bf16[384,1024]{1,0:T(8,128)(2,1)S(1)}, bf16[384,1024]{1,0:T(8,128)(2,1)S(1)}, u32[]{:S(2)}, u32[]{:S(2)}) collective-permute-start(bf16[384,1024]{1,0:T(8,128)(2,1)S(1)} %get-tuple-element.44), channel_id=1, source_target_pairs={{0,1},{1,0},{2,3},{3,2},{4,5},{5,4},{6,7},{7,6},{8,9},{9,8},{10,11... | collective-permute-start | bytes 2359304 | tf_op jit(solution)/shard_map/ppermute | solution.py:137
  52.7 8.7 %collective-permute-start.23 = (bf16[704,256]{1,0:T(8,128)(2,1)S(1)}, bf16[704,256]{1,0:T(8,128)(2,1)S(1)}, u32[]{:S(2)}, u32[]{:S(2)}) collective-permute-start(bf16[704,256]{1,0:T(8,128)(2,1)S(1)} %add_convert_fusion.2), channel_id=1, source_target_pairs={{0,8},{1,25},{8,16},{9,1},{16,24},{17,9},{24,0},{25,17},{2,10},{3,... | collective-permute-start | bytes 1081352 | tf_op jit(solution)/shard_map/ppermute | solution.py:188
  53.5 11.1 %collective-permute-start.26 = (bf16[352,256]{1,0:T(8,128)(2,1)S(1)}, bf16[352,256]{1,0:T(8,128)(2,1)S(1)}, u32[]{:S(2)}, u32[]{:S(2)}) collective-permute-start(bf16[352,256]{1,0:T(8,128)(2,1)S(1)} %get-tuple-element.54), channel_id=1, source_target_pairs={{8,0},{25,1},{16,8},{1,9},{24,16},{9,17},{0,24},{17,25},{10,2},{27... | collective-permute-start | bytes 540680 | tf_op jit(solution)/shard_map/ppermute | solution.py:187
  56.1 8.5 %collective-permute-start.28 = (bf16[352,256]{1,0:T(8,128)(2,1)S(1)}, bf16[352,256]{1,0:T(8,128)(2,1)S(1)}, u32[]{:S(2)}, u32[]{:S(2)}) collective-permute-start(bf16[352,256]{1,0:T(8,128)(2,1)S(1)} %add_convert_fusion.6), channel_id=1, source_target_pairs={{0,8},{1,25},{8,16},{9,1},{16,24},{17,9},{24,0},{25,17},{2,10},{3,... | collective-permute-start | bytes 540680 | tf_op jit(solution)/shard_map/ppermute | solution.py:188
  61.5 9.2 %collective-permute-start.24 = (bf16[704,256]{1,0:T(8,128)(2,1)S(1)}, bf16[704,256]{1,0:T(8,128)(2,1)S(1)}, u32[]{:S(2)}, u32[]{:S(2)}) collective-permute-start(bf16[704,256]{1,0:T(8,128)(2,1)S(1)} %add_convert_fusion.1), channel_id=1, source_target_pairs={{0,32},{1,97},{32,0},{33,65},{64,96},{65,33},{96,64},{97,1},{2,34}... | collective-permute-start | bytes 1081352 | tf_op jit(solution)/shard_map/ppermute | solution.py:193
  63.7 6.9 %collective-permute-start.19 = (bf16[96,1024]{1,0:T(8,128)(2,1)S(1)}, bf16[96,1024]{1,0:T(8,128)(2,1)S(1)}, u32[]{:S(2)}, u32[]{:S(2)}) collective-permute-start(bf16[96,1024]{1,0:T(8,128)(2,1)S(1)} %get-tuple-element.48), channel_id=1, source_target_pairs={{0,2},{1,7},{2,4},{3,1},{4,6},{5,3},{6,0},{7,5},{8,10},{9,15},{10,... | collective-permute-start | bytes 589832 | tf_op jit(solution)/shard_map/ppermute | solution.py:186
  64.6 11.5 %collective-permute-start.29 = (bf16[352,256]{1,0:T(8,128)(2,1)S(1)}, bf16[352,256]{1,0:T(8,128)(2,1)S(1)}, u32[]{:S(2)}, u32[]{:S(2)}) collective-permute-start(bf16[352,256]{1,0:T(8,128)(2,1)S(1)} %add_convert_fusion.5), channel_id=1, source_target_pairs={{0,32},{1,97},{32,0},{33,65},{64,96},{65,33},{96,64},{97,1},{2,34}... | collective-permute-start | bytes 540680 | tf_op jit(solution)/shard_map/ppermute | solution.py:193
  65.4 14.5 %collective-permute-start.18 = (bf16[96,1024]{1,0:T(8,128)(2,1)S(1)}, bf16[96,1024]{1,0:T(8,128)(2,1)S(1)}, u32[]{:S(2)}, u32[]{:S(2)}) collective-permute-start(bf16[96,1024]{1,0:T(8,128)(2,1)S(1)} %get-tuple-element.46), channel_id=1, source_target_pairs={{2,0},{7,1},{4,2},{1,3},{6,4},{3,5},{0,6},{5,7},{10,8},{15,9},{12,... | collective-permute-start | bytes 589832 | tf_op jit(solution)/shard_map/ppermute | solution.py:187
  70.7 9.3 %collective-permute-start.20 = (bf16[96,1024]{1,0:T(8,128)(2,1)S(1)}, bf16[96,1024]{1,0:T(8,128)(2,1)S(1)}, u32[]{:S(2)}, u32[]{:S(2)}) collective-permute-start(bf16[96,1024]{1,0:T(8,128)(2,1)S(1)} %add_convert_fusion.3), channel_id=1, source_target_pairs={{0,2},{1,7},{2,4},{3,1},{4,6},{5,3},{6,0},{7,5},{8,10},{9,15},{10,... | collective-permute-start | bytes 589832 | tf_op jit(solution)/shard_map/ppermute | solution.py:188
  70.9 12.6 %collective-permute-start.25 = (bf16[704,256]{1,0:T(8,128)(2,1)S(1)}, bf16[704,256]{1,0:T(8,128)(2,1)S(1)}, u32[]{:S(2)}, u32[]{:S(2)}) collective-permute-start(bf16[704,256]{1,0:T(8,128)(2,1)S(1)} %add_convert_fusion.a), channel_id=1, source_target_pairs={{0,96},{1,33},{32,64},{33,1},{64,32},{65,97},{96,0},{97,65},{2,98}... | collective-permute-start | bytes 1081352 | tf_op jit(solution)/shard_map/ppermute | solution.py:194
  76.2 7.3 %collective-permute-start.30 = (bf16[352,256]{1,0:T(8,128)(2,1)S(1)}, bf16[352,256]{1,0:T(8,128)(2,1)S(1)}, u32[]{:S(2)}, u32[]{:S(2)}) collective-permute-start(bf16[352,256]{1,0:T(8,128)(2,1)S(1)} %add_convert_fusion.4.down_a), channel_id=1, source_target_pairs={{0,96},{1,33},{32,64},{33,1},{64,32},{65,97},{96,0},{97,65},{2,98}... | collective-permute-start | bytes 540680 | tf_op jit(solution)/shard_map/ppermute | solution.py:194
